TPU v7x, 256 devices: a whole 4x4x8 slice. The times are simulated.
256 devices in a mesh: ep: 32 (over z, x), tp: 8 (over y, core).
Axes of the slice: x: 4, y: 4, z: 8, core: 2. Of those that a mesh axis runs over, the one named last changes fastest.
Arguments:
- tokens: bfloat16 [1024, 2048], P('ep'), may hold values from -24 to 24
- norm_gain: float32 [2048], replicated, may hold values from 0.1 to 1.9
- post_gain: float32 [2048], replicated, may hold values from 0.1 to 1.9
- w_query: bfloat16 [2048, 2048], P(None, 'tp'), may hold values from -0.125 to 0.125
- w_key: bfloat16 [2048, 512], P(None, 'tp'), may hold values from -0.125 to 0.125
- w_value: bfloat16 [2048, 512], P(None, 'tp'), may hold values from -0.125 to 0.125
- w_forget: bfloat16 [2048, 32], replicated, may hold values from -0.25 to 0.25
- w_output: bfloat16 [2048, 2048], P('tp'), may hold values from -0.125 to 0.125
- key_cache: bfloat16 [1024, 8, 64, 1024], P('ep', 'tp'), may hold values from -660 to 660
- value_cache: bfloat16 [1024, 8, 64, 1024], P('ep', 'tp'), may hold values from -6 to 6
- gate_cache: float32 [1024, 32, 1024], P('ep', 'tp'), may hold values from -176.08 to 0, as said below
- lengths: int32 [1024], P('ep'), may hold values from 256 to 1024
- routes: int32 [1024, 2], P('ep'), may hold values from 0 to 31, all different within a row; in each aligned block of 32 rows (0 to 31, 32 to 63, ...) at most 4 rows name the same one
- route_logits: float32 [1024, 2], P('ep'), may hold values from -6 to 6
- w_gate: bfloat16 [32, 2048, 3584], P('ep', None, 'tp'), may hold values from -0.125 to 0.125
- w_up: bfloat16 [32, 2048, 3584], P('ep', None, 'tp'), may hold values from -0.125 to 0.125
- w_down: bfloat16 [32, 3584, 2048], P('ep', 'tp'), may hold values from -0.09375 to 0.09375
Outputs:
- layer_out: bfloat16 [1024, 2048], P('ep', 'tp')
Inputs may be any that keep to these rules, and one draw needn't show every extreme that they name: `routes`: each row names 2 different experts. The rows of one index of ep name any one expert at most 4 times, and in every draw some index of ep names some expert exactly 4 times. `gate_cache`: cumulative sums of negative log forget gates along positions: nonincreasing along the last dimension. `lengths`: the new token follows the valid positions of its sequence.
All inputs are finite; a program needn't handle non-finite values.
Results may differ from a plain program's by a relative error of at most 0.011.
Values may be sent and summed in bfloat16 or wider, within the bound.
A program may use at most 64 MiB of HBM per device.

v0:
```python
import jax
import jax.numpy as jnp
from jax import lax
from jax.sharding import PartitionSpec as P

epsilon = 1e-06


def copy_for_each(array, axis):
    copies = jnp.broadcast_to(array, (lax.axis_size(axis), *array.shape))
    return lax.all_to_all(copies, axis, split_axis=0, concat_axis=0, tiled=True)


def over_copies(array, axis):
    everything = copy_for_each(array, axis)
    return jnp.sum(everything.astype(jnp.float32), axis=0)


def cut_along(array, dim, count):
    shape = array.shape
    blocks = array.reshape(*shape[:dim], count, shape[dim] // count, *shape[dim + 1 :])
    return jnp.moveaxis(blocks, dim, 0)


def sum_at_owner(array, axis, dim):
    blocks = cut_along(array, dim, lax.axis_size(axis))
    arrived = lax.all_to_all(blocks, axis, split_axis=0, concat_axis=0, tiled=True)
    return arrived.astype(jnp.float32).sum(axis=0)


def body(
    tokens,
    norm_gain,
    post_gain,
    w_query,
    w_key,
    w_value,
    w_forget,
    w_output,
    key_cache,
    value_cache,
    gate_cache,
    lengths,
    routes,
    route_logits,
    w_gate,
    w_up,
    w_down,
):
    ep_count = lax.axis_size("ep")
    tp_count = lax.axis_size("tp")
    tp_index = lax.axis_index("tp")
    seq_count, width = tokens.shape
    kv_local, head_dim, cache_span = (key_cache.shape[1], key_cache.shape[2], key_cache.shape[3])
    heads_local = gate_cache.shape[1]
    group_size = heads_local // kv_local
    own_width = width // tp_count
    column_start = tp_index * own_width
    tokens_wide = tokens.astype(jnp.float32)
    normed = (
        tokens_wide
        * lax.rsqrt(jnp.mean(tokens_wide * tokens_wide, axis=-1, keepdims=True) + epsilon)
        * norm_gain
    ).astype(jnp.bfloat16)
    forget_columns = lax.dynamic_slice_in_dim(w_forget, tp_index * heads_local, heads_local, 1)
    log_forget = jax.nn.log_sigmoid(
        jnp.dot(normed, forget_columns, preferred_element_type=jnp.float32)
    )
    query_vector = jnp.dot(normed, w_query, preferred_element_type=jnp.float32).astype(jnp.bfloat16)
    fresh_key = jnp.dot(normed, w_key, preferred_element_type=jnp.float32).astype(jnp.bfloat16)
    value_new = jnp.dot(normed, w_value, preferred_element_type=jnp.float32).astype(jnp.bfloat16)
    query_vector = query_vector.reshape(seq_count, kv_local, group_size, head_dim)
    fresh_key = fresh_key.reshape(seq_count, kv_local, head_dim)
    value_new = value_new.reshape(seq_count, kv_local, head_dim)
    score_scale = head_dim ** (-0.5)
    past_scores = jnp.einsum(
        "bkgd,bkdl->bkgl", query_vector, key_cache, preferred_element_type=jnp.float32
    ).reshape(seq_count, heads_local, cache_span)
    cache_position = lax.broadcasted_iota(jnp.int32, (1, 1, cache_span), 2)
    last_index = (lengths - 1)[:, None, None]
    latest = jnp.sum(jnp.where(cache_position == last_index, gate_cache, 0.0), axis=-1)
    past_scores = past_scores * score_scale + (latest + log_forget)[:, :, None] - gate_cache
    past_scores = jnp.where(cache_position < lengths[:, None, None], past_scores, -jnp.inf)
    new_score = (
        jnp.einsum(
            "rlse,rle->rls", query_vector, fresh_key, preferred_element_type=jnp.float32
        ).reshape(seq_count, heads_local)
        * score_scale
    )
    peak_score = jnp.maximum(jnp.max(past_scores, axis=-1), new_score)
    past_exp = jnp.exp(past_scores - peak_score[:, :, None])
    new_exp = jnp.exp(new_score - peak_score)
    denominator = jnp.sum(past_exp, axis=-1) + new_exp
    past_prob = (past_exp / denominator[:, :, None]).astype(jnp.bfloat16)
    new_prob = (new_exp / denominator).astype(jnp.bfloat16)
    mixed_heads = jnp.einsum(
        "bkgl,bkdl->bkgd",
        past_prob.reshape(seq_count, kv_local, group_size, cache_span),
        value_cache,
        preferred_element_type=jnp.float32,
    )
    mixed_heads = mixed_heads + new_prob.reshape(seq_count, kv_local, group_size)[
        :, :, :, None
    ].astype(jnp.float32) * value_new[:, :, None, :].astype(jnp.float32)
    attended = mixed_heads.astype(jnp.bfloat16).reshape(seq_count, heads_local * head_dim)
    partial_value = jnp.dot(attended, w_output, preferred_element_type=jnp.float32).astype(
        jnp.bfloat16
    )
    attention = over_copies(partial_value, "tp").astype(jnp.float32)
    stream = tokens_wide + attention
    expert_input = (
        stream * lax.rsqrt(jnp.mean(stream * stream, axis=-1, keepdims=True) + epsilon) * post_gain
    ).astype(jnp.bfloat16)
    residual = lax.dynamic_slice_in_dim(stream, column_start, own_width, 1)
    route_width = routes.shape[1]
    route_count = seq_count * route_width
    capacity = 2 * seq_count * route_width // ep_count
    slot_count = ep_count * capacity
    flat_routes = routes.reshape(route_count)
    expert_onehot = (
        flat_routes[:, None] == lax.broadcasted_iota(jnp.int32, (1, ep_count), 1)
    ).astype(jnp.int32)
    route_rank = jnp.sum(jnp.cumsum(expert_onehot, axis=0) * expert_onehot, axis=1) - 1
    slot_index = flat_routes * capacity + route_rank
    slot_onehot = (
        slot_index[:, None] == lax.broadcasted_iota(jnp.int32, (1, slot_count), 1)
    ).astype(jnp.float32)
    token_onehot = (
        lax.broadcasted_iota(jnp.int32, (route_count, 1), 0) // route_width
        == lax.broadcasted_iota(jnp.int32, (1, seq_count), 1)
    ).astype(jnp.float32)
    dispatch = jnp.dot(slot_onehot.T, token_onehot).astype(jnp.bfloat16)
    packed = jnp.dot(dispatch, expert_input, preferred_element_type=jnp.float32).astype(
        jnp.bfloat16
    )
    sent_width = packed.shape[1]
    arrived = lax.all_to_all(
        packed.reshape(ep_count, capacity, sent_width),
        "ep",
        split_axis=0,
        concat_axis=0,
        tiled=True,
    )
    expert_rows = arrived.reshape(slot_count, sent_width)
    gate_act = jnp.dot(expert_rows, w_gate[0], preferred_element_type=jnp.float32)
    upper = jnp.dot(expert_rows, w_up[0], preferred_element_type=jnp.float32)
    hidden_act = (jax.nn.silu(gate_act) * upper).astype(jnp.bfloat16)
    down_part = jnp.dot(hidden_act, w_down[0], preferred_element_type=jnp.float32).astype(
        jnp.bfloat16
    )
    expert_out = sum_at_owner(down_part, "tp", 1).astype(jnp.bfloat16)
    returned = lax.all_to_all(
        expert_out.reshape(ep_count, capacity, own_width),
        "ep",
        split_axis=0,
        concat_axis=0,
        tiled=True,
    )
    route_weight = jax.nn.softmax(route_logits, axis=-1).reshape(route_count)
    combine = jnp.dot(
        token_onehot.T, slot_onehot * route_weight[:, None], precision=lax.Precision.HIGHEST
    )
    expert_mix = jnp.dot(
        combine,
        returned.reshape(slot_count, own_width).astype(jnp.float32),
        precision=lax.Precision.HIGHEST,
    )
    return (residual + expert_mix).astype(jnp.bfloat16)


def solution(mesh):
    in_specs = (
        P("ep", None),
        P(),
        P(),
        P(None, "tp"),
        P(None, "tp"),
        P(None, "tp"),
        P(),
        P("tp", None),
        P("ep", "tp", None, None),
        P("ep", "tp", None, None),
        P("ep", "tp", None),
        P("ep"),
        P("ep", None),
        P("ep", None),
        P("ep", None, "tp"),
        P("ep", None, "tp"),
        P("ep", "tp", None),
    )
    out_specs = P("ep", "tp")
    return jax.shard_map(body, mesh=mesh, in_specs=in_specs, out_specs=out_specs, check_vma=False)
```

profile of v0, /device:TPU:1, one launch (start us, length us, event | category | flops | bytes accessed | tf_op | source)
XLA Modules:
  0.0 101.1 jit_solution(10886964392993682027)
XLA Ops:
  0.0 0.8 broadcast_add_fusion
  0.8 0.8 iota_compare_fusion.1
  1.6 1.0 %fusion.39 = f32[32]{0:T(128)S(1)} fusion(bf16[32,2048]{1,0:T(8,128)(2,1)} %param.17), kind=kLoop, calls=%fused_computation.38 | loop fusion | flops 196576 | bytes 131200 | tf_op jit(solution)/shard_map/reduce_sum | solution.py:62
  2.8 1.3 %select_reduce_fusion = f32[32,4]{1,0:T(8,128)S(1)} fusion(f32[32,4,1024]{2,1,0:T(4,128)} %param.27, pred[32,1024]{1,0:T(8,128)(4,1)S(1)} %iota_compare_fusion), kind=kLoop, calls=%fused_computation.32 | loop fusion | flops 262016 | bytes 557568 | tf_op jit(solution)/shard_map/reduce_sum | solution.py:81
  4.2 1.2 %fusion.69 = f32[32,4]{0,1:T(4,128)S(1)} fusion(f32[32,4]{0,1:T(4,128)S(1)} %copy.29, bf16[2048,32]{0,1:T(8,128)(2,1)} %param.23, s32[]{:T(128)S(6)} %select_n.31, bf16[32,2048]{1,0:T(8,128)(2,1)} %param.17, f32[2048]{0:T(1024)} %param.18, f32[32]{0:T(128)S(1)} %add_rsqrt_fusion.1), kind=kOutput, calls=%fused_computation.78 | convolution fusion | flops 787584 | bytes 156804 | tf_op jit(solution)/shard_map/dot_general | solution.py:67
  5.4 1.7 %convolution_convert_fusion.3 = bf16[32,256]{1,0:T(8,128)(2,1)S(1)} fusion(bf16[2048,256]{1,0:T(8,128)(2,1)} %param.20, bf16[32,2048]{1,0:T(8,128)(2,1)} %param.17, f32[2048]{0:T(1024)} %param.18, f32[32]{0:T(128)S(1)} %add_rsqrt_fusion.1), kind=kOutput, calls=%fused_computation.23 | convolution fusion | flops 33824768 | bytes 1204352 | tf_op jit(solution)/shard_map/dot_general | solution.py:69
  7.2 0.3 fusion.37
  7.5 0.2 fusion.64
  7.7 3.1 %fusion.81 = (f32[32,4]{1,0:T(8,128)S(1)}, f32[32,4,1024]{2,1,0:T(4,128)S(1)}) fusion(f32[32,4,1024]{2,1,0:T(4,128)S(1)} %copy-done.2, f32[32,4]{1,0:T(8,128)S(1)} %copy.30, bf16[32,4,64]{2,1,0:T(4,128)(2,1)S(1)} %reshape.193, bf16[32,1,64,1024]{3,2,1,0:T(8,128)(2,1)} %param.25, pred[32,1024]{1,0:T(8,128)(4,1)S(1)} %iota_compare_fusion.1), kind=kOutput, calls=%fused_computation.93 | convolution fusion | flops 17432448 | bytes 5293056 | tf_op jit(solution)/shard_map/bkgd,bkdl->bkgl/dot_general | solution.py:76
  10.8 0.3 fusion.38
  11.2 0.3 fusion.36
  11.5 1.3 %fusion.29 = bf16[32,4,64]{2,1,0:T(4,128)(2,1)S(1)} fusion(bf16[32,1,64,1024]{3,2,1,0:T(8,128)(2,1)S(1)} %copy-done.10, f32[32,4,1024]{2,1,0:T(4,128)S(1)} %get-tuple-element.10, f32[32,4]{1,0:T(8,128)S(1)} %get-tuple-element.8, f32[32,4]{1,0:T(8,128)S(1)} %multiply_maximum_fusion, f32[32,64]{1,0:T(8,128)S(1)} %fusion.36, f32[32,4]{1,0:T(8,128)S(1)} %get-tuple-element.7), kind=kOutput, calls=%fused_computation.19 | convolution fusion | flops 17195008 | bytes 4744704 | tf_op jit(solution)/shard_map/bkgl,bkdl->bkgd/dot_general | solution.py:96
  12.8 0.3 convolution_convert_fusion.2
  13.1 1.1 %broadcast_in_dim.39 = bf16[8,32,2048]{2,1,0:T(8,128)(2,1)} broadcast(bf16[32,2048]{1,0:T(8,128)(2,1)S(1)} %convolution_convert_fusion.2), dimensions={1,2} | broadcast | bytes 1179648 | tf_op jit(solution)/shard_map/broadcast_in_dim | solution.py:10
  14.3 6.8 %all-to-all-start = ((bf16[8,32,2048]{2,1,0:T(8,128)(2,1)}), bf16[8,32,2048]{2,1,0:T(8,128)(2,1)S(1)}, u32[]{:S(2)}, u32[]{:S(2)}) async-start(bf16[8,32,2048]{2,1,0:T(8,128)(2,1)} %broadcast_in_dim.39), calls=%async_computation | async-start | bytes 2097152 | tf_op jit(solution)/shard_map/all_to_all | solution.py:11
  21.4 0.2 select_reduce_fusion.1
  21.6 14.4 %all-to-all-done = bf16[8,32,2048]{2,1,0:T(8,128)(2,1)S(1)} async-done(((bf16[8,32,2048]{2,1,0:T(8,128)(2,1)}), bf16[8,32,2048]{2,1,0:T(8,128)(2,1)S(1)}, u32[]{:S(2)}, u32[]{:S(2)}) %all-to-all-start) | async-done | bytes 1048608 | tf_op jit(solution)/shard_map/all_to_all | solution.py:11
  36.2 0.1 multiply_reduce_fusion
  36.4 0.7 copy-done.3
  37.0 0.6 convolution_convert_fusion.1
  37.6 0.2 reshape.198
  37.8 25.5 %all_to_all.20 = bf16[32,4,2048]{2,1,0:T(4,128)(2,1)S(1)} all-to-all(bf16[32,4,2048]{2,1,0:T(4,128)(2,1)S(1)} %reshape.198), channel_id=1, replica_groups=mesh['ep'=32,'tp'=8] {'ep'}, dimensions={0} | all-to-all | bytes 1048576 | tf_op jit(solution)/shard_map/all_to_all | solution.py:137
  63.4 2.1 %fusion.7 = f32[128,448]{0,1:T(8,128)S(1)} fusion(bf16[128,2048]{1,0:T(8,128)(2,1)S(1)} %reshape.199, bf16[1,2048,448]{1,2,0:T(8,128)(2,1)} %param.31), kind=kOutput, calls=%fused_computation.11 | convolution fusion | flops 234881024 | bytes 2588672 | tf_op jit(solution)/shard_map/dot_general | solution.py:145
  65.6 3.0 %convolution_convert_fusion = bf16[128,2048]{1,0:T(8,128)(2,1)S(1)} fusion(bf16[1,448,2048]{2,1,0:T(8,128)(2,1)S(1)} %copy-done, bf16[128,2048]{1,0:T(8,128)(2,1)S(1)} %reshape.199, bf16[1,2048,448]{1,2,0:T(8,128)(2,1)} %param.32, f32[128,448]{0,1:T(8,128)S(1)} %fusion.7), kind=kOutput, calls=%fused_computation.4 | convolution fusion | flops 470368256 | bytes 4947968 | tf_op jit(solution)/shard_map/dot_general | solution.py:148
  68.7 0.8 copy.40
  69.5 6.7 %all-to-all-start.2 = ((bf16[8,128,256]{2,1,0:T(8,128)(2,1)}), bf16[8,128,256]{2,1,0:T(8,128)(2,1)S(1)}, u32[]{:S(2)}, u32[]{:S(2)}) async-start(bf16[8,128,256]{2,1,0:T(8,128)(2,1)} %bitcast.56), calls=%async_computation.2 | async-start | bytes 1048576 | tf_op jit(solution)/shard_map/all_to_all | solution.py:27
  76.5 9.1 %all-to-all-done.2 = bf16[8,128,256]{2,1,0:T(8,128)(2,1)S(1)} async-done(((bf16[8,128,256]{2,1,0:T(8,128)(2,1)}), bf16[8,128,256]{2,1,0:T(8,128)(2,1)S(1)}, u32[]{:S(2)}, u32[]{:S(2)}) %all-to-all-start.2) | async-done | bytes 524320 | tf_op jit(solution)/shard_map/all_to_all | solution.py:27
  85.7 0.6 reshape.201
  86.3 4.4 %all-to-all-start.3 = ((bf16[32,4,256]{2,1,0:T(4,128)(2,1)}), bf16[32,4,256]{2,1,0:T(4,128)(2,1)S(1)}, u32[]{:S(2)}, u32[]{:S(2)}) async-start(bf16[32,4,256]{2,1,0:T(4,128)(2,1)} %reshape.201), calls=%async_computation.3 | async-start | bytes 131072 | tf_op jit(solution)/shard_map/all_to_all | solution.py:152
  90.7 0.3 fusion.52
  90.9 8.6 %all-to-all-done.3 = bf16[32,4,256]{2,1,0:T(4,128)(2,1)S(1)} async-done(((bf16[32,4,256]{2,1,0:T(4,128)(2,1)}), bf16[32,4,256]{2,1,0:T(4,128)(2,1)S(1)}, u32[]{:S(2)}, u32[]{:S(2)}) %all-to-all-start.3) | async-done | bytes 65568 | tf_op jit(solution)/shard_map/all_to_all | solution.py:152
  99.5 1.5 %fusion.35 = bf16[32,256]{1,0:T(8,128)(2,1)} fusion(f32[32,128]{1,0:T(8,128)S(1)} %fusion.52, bf16[128,256]{1,0:T(8,128)(2,1)S(1)} %reshape.202, f32[32,2048]{1,0:T(8,128)} %copy-done.3, s32[]{:T(128)S(6)} %select_n.34), kind=kOutput, calls=%fused_computation.22 | convolution fusion | flops 12599296 | bytes 131076 | tf_op jit(solution)/shard_map/dot_general | solution.py:163
  (46 shorter events, 1.6 us)
Async XLA Ops:
  0.0 65.6 %copy-start = (bf16[1,448,2048]{2,1,0:T(8,128)(2,1)S(1)}, bf16[1,448,2048]{2,1,0:T(8,128)(2,1)}, u32[]{:S(2)}) copy-start(bf16[1,448,2048]{2,1,0:T(8,128)(2,1)} %param.33) | copy-start | bytes 5505028
  0.0 7.2 %copy-start.1 = (bf16[32,2048]{1,0:T(8,128)(2,1)S(1)}, bf16[32,2048]{1,0:T(8,128)(2,1)}, u32[]{:S(2)}) copy-start(bf16[32,2048]{1,0:T(8,128)(2,1)} %param.17) | copy-start | bytes 393220
  0.0 7.6 %copy-start.2 = (f32[32,4,1024]{2,1,0:T(4,128)S(1)}, f32[32,4,1024]{2,1,0:T(4,128)}, u32[]{:S(2)}) copy-start(f32[32,4,1024]{2,1,0:T(4,128)} %param.27) | copy-start | bytes 1572868
  0.0 7.2 %copy-start.6 = (f32[2048]{0:T(1024)S(1)}, f32[2048]{0:T(1024)}, u32[]{:S(2)}) copy-start(f32[2048]{0:T(1024)} %param.18) | copy-start | bytes 24580
  0.0 7.2 %copy-start.11 = (bf16[2048,64]{0,1:T(8,128)(2,1)S(1)}, bf16[2048,64]{0,1:T(8,128)(2,1)}, u32[]{:S(2)}) copy-start(bf16[2048,64]{0,1:T(8,128)(2,1)} %param.21) | copy-start | bytes 786436
  7.7 3.5 %copy-start.5 = (bf16[2048,64]{0,1:T(8,128)(2,1)S(1)}, bf16[2048,64]{0,1:T(8,128)(2,1)}, u32[]{:S(2)}) copy-start(bf16[2048,64]{0,1:T(8,128)(2,1)} %param.22) | copy-start | bytes 786436
  7.7 3.8 %copy-start.10 = (bf16[32,1,64,1024]{3,2,1,0:T(8,128)(2,1)S(1)}, bf16[32,1,64,1024]{3,2,1,0:T(8,128)(2,1)}, u32[]{:S(2)}) copy-start(bf16[32,1,64,1024]{3,2,1,0:T(8,128)(2,1)} %param.26) | copy-start | bytes 12582916
  11.4 1.4 %copy-start.4 = (bf16[256,2048]{1,0:T(8,128)(2,1)S(1)}, bf16[256,2048]{1,0:T(8,128)(2,1)}, u32[]{:S(2)}) copy-start(bf16[256,2048]{1,0:T(8,128)(2,1)} %param.24) | copy-start | bytes 3145732
  13.1 7.9 %copy-start.9 = (s32[32,2]{0,1:T(2,128)S(1)}, s32[32,2]{0,1:T(2,128)}, u32[]{:S(2)}) copy-start(s32[32,2]{0,1:T(2,128)} %param.29) | copy-start | bytes 772
  14.3 22.8 %copy-start.8 = (f32[2048]{0:T(1024)S(1)}, f32[2048]{0:T(1024)}, u32[]{:S(2)}) copy-start(f32[2048]{0:T(1024)} %param.19) | copy-start | bytes 24580
  14.3 21.8 %all-to-all-start = ((bf16[8,32,2048]{2,1,0:T(8,128)(2,1)}), bf16[8,32,2048]{2,1,0:T(8,128)(2,1)S(1)}, u32[]{:S(2)}, u32[]{:S(2)}) async-start(bf16[8,32,2048]{2,1,0:T(8,128)(2,1)} %broadcast_in_dim.39), calls=%async_computation | async-start | bytes 2097152 | tf_op jit(solution)/shard_map/all_to_all | solution.py:11
  36.3 0.7 copy-start.3
  68.6 7.6 %copy-start.7 = (f32[32,2]{0,1:T(2,128)S(1)}, f32[32,2]{0,1:T(2,128)}, u32[]{:S(2)}) copy-start(f32[32,2]{0,1:T(2,128)} %param.30) | copy-start | bytes 772
  69.5 16.1 %all-to-all-start.2 = ((bf16[8,128,256]{2,1,0:T(8,128)(2,1)}), bf16[8,128,256]{2,1,0:T(8,128)(2,1)S(1)}, u32[]{:S(2)}, u32[]{:S(2)}) async-start(bf16[8,128,256]{2,1,0:T(8,128)(2,1)} %bitcast.56), calls=%async_computation.2 | async-start | bytes 1048576 | tf_op jit(solution)/shard_map/all_to_all | solution.py:27
  86.3 13.2 %all-to-all-start.3 = ((bf16[32,4,256]{2,1,0:T(4,128)(2,1)}), bf16[32,4,256]{2,1,0:T(4,128)(2,1)S(1)}, u32[]{:S(2)}, u32[]{:S(2)}) async-start(bf16[32,4,256]{2,1,0:T(4,128)(2,1)} %reshape.201), calls=%async_computation.3 | async-start | bytes 131072 | tf_op jit(solution)/shard_map/all_to_all | solution.py:152
where the time goes:
time: 102 us; the launch traced here: 101 us
  waiting for transfers between devices  32.1 us (31%)
  blocking collectives  25.5 us (25%)
  starting transfers between devices  17.9 us (18%)
  matrix products  15.7 us (15%)
  other arithmetic  5.17 us (5%)
  local copies, waits for them, and re-layouts  4.44 us (4%)
    all_to_all x1, blocking collectives, body(): lax.all_to_all(packed.reshape(ep_count, capacity, sent_width), 'ep', spli...  25.5 us
    all_to_all x1, waiting for transfers between devices, copy_for_each(): return lax.all_to_all(copies, axis, split_axis=0, concat_axis=0, tiled=True)  14.4 us
    all_to_all x1, waiting for transfers between devices, sum_at_owner(): lax.all_to_all(blocks, axis, split_axis=0, concat_axis=0, tiled=True)  9.11 us
    all_to_all x1, waiting for transfers between devices, body(): lax.all_to_all(expert_out.reshape(ep_count, capacity, own_width), 'ep', s...  8.57 us
    all_to_all x1, starting transfers between devices, copy_for_each(): return lax.all_to_all(copies, axis, split_axis=0, concat_axis=0, tiled=True)  6.79 us
    all_to_all x1, starting transfers between devices, sum_at_owner(): lax.all_to_all(blocks, axis, split_axis=0, concat_axis=0, tiled=True)  6.72 us
    all_to_all x1, starting transfers between devices, body(): lax.all_to_all(expert_out.reshape(ep_count, capacity, own_width), 'ep', s...  4.37 us
    dot_general x1, matrix products, body(): jnp.einsum('bkgd,bkdl->bkgl', query_vector, key_cache, preferred_element_...  3.14 us
  transfers between devices with their start and end apart: 3, of which 3 were waited for; matrix products, arithmetic and copies ran while one was open for 1% of the time, Pallas kernels for 0%

commit v1 on v0

v1 whole, which is shorter than its diff:
```python
import functools

import jax
import jax.numpy as jnp
from jax import lax
from jax.experimental import pallas as pl
from jax.experimental.pallas import tpu as pltpu
from jax.sharding import PartitionSpec as P

f32 = jnp.float32
bf16 = jnp.bfloat16
MESH = pl.DeviceIdType.MESH
EPSILON = 1e-06


def mm(a, b):
    return jnp.dot(a, b, preferred_element_type=f32)


def mm_nt(a, b):
    return lax.dot_general(a, b, (((1,), (1,)), ((), ())), preferred_element_type=f32)


def iota(shape, dim):
    return lax.broadcasted_iota(jnp.int32, shape, dim)


def interleave(even, odd):
    low = iota(even.shape, 1) < 4
    first = jnp.where(low, even, pltpu.roll(odd, 4, 1))
    second = jnp.where(low, pltpu.roll(even, 4, 1), odd)
    return first, second


def kernel(n_ep, n_tp, *refs):
    hbm = refs[:17]
    out_ref = refs[17]
    (
        tok, ngain, pgain, wq, wk, wv, wf, wo, keys, vals, gates, lens, routes, logits, wg, wu, wd,
    ) = refs[18:35]
    (
        probs, asend, arecv, packed, arrived, blocks, psend, precv, tsend, trecv, ret_send, ret,
        load_sem, a_s, a_r, d_s, d_r, g_s, g_r, p_s, p_r, t_s, t_r, b_s, b_r,
    ) = refs[35:]
    n_y = n_tp // 2
    me = lax.axis_index("ep")
    t = lax.axis_index("tp")
    y = t // 2
    c = t % 2
    seqs, width = tok.shape
    heads = gates.shape[1]
    rows = seqs * heads
    span = keys.shape[1]
    hd = keys.shape[0] // seqs
    own = width // n_tp

    def tp_at(dy, dc):
        return ((y + dy) % n_y) * 2 + (c if dc == 0 else 1 - c)

    def tp_from(dy, dc):
        return ((y + n_y - dy) % n_y) * 2 + (c if dc == 0 else 1 - c)

    def load(n, dst, part=None):
        src = hbm[n]
        if part is not None:
            src, dst = src.at[part], dst.at[part]
        load.count += 1
        copy = pltpu.make_async_copy(src, dst, load_sem.at[load.count - 1])
        copy.start()
        return copy

    load.count = 0
    group = 4
    n_groups = seqs // group
    gr = group * heads
    gk = group * hd
    chunk = 2
    slices = [pl.ds(n * chunk * gk, chunk * gk) for n in range(n_groups // chunk)]
    l_tok = load(0, tok)
    l_ngain = load(1, ngain)
    l_wq = load(3, wq)
    l_wk = load(4, wk)
    l_wv = load(5, wv)
    l_wf = load(6, wf)
    l_small = [load(11, lens), load(12, routes), load(13, logits), load(2, pgain)]
    l_keys = [load(8, keys, s) for s in slices]
    l_gates = load(10, gates)
    l_vals = [load(9, vals, s) for s in slices]
    l_wo = load(7, wo)
    l_wg = load(14, wg)
    l_wu = load(15, wu)
    l_wd = load(16, wd)

    barrier = pltpu.get_barrier_semaphore()
    for k in range(1, n_ep):
        pl.semaphore_signal(
            barrier, inc=1, device_id={"ep": (me + k) % n_ep}, device_id_type=MESH
        )
    for n in range(1, n_tp):
        pl.semaphore_signal(
            barrier, inc=1, device_id={"tp": tp_at(n // 2, n % 2)}, device_id_type=MESH
        )

    l_tok.wait()
    l_ngain.wait()
    x = tok[...].astype(f32)
    normed = x * lax.rsqrt(jnp.mean(x * x, axis=-1, keepdims=True) + EPSILON) * ngain[...]
    repeat = (iota((rows, seqs), 0) // heads) == iota((rows, seqs), 1)
    normed = mm(repeat.astype(bf16), normed.astype(bf16)).astype(bf16)
    l_wq.wait()
    q = mm(normed, wq[...]).astype(bf16).astype(f32)
    l_wk.wait()
    k_new = mm_nt(normed, wk[...]).astype(bf16).astype(f32)
    l_wv.wait()
    v_new = mm_nt(normed, wv[...]).astype(bf16).astype(f32)
    l_wf.wait()
    forget = mm_nt(normed, wf[...])
    for copy in l_small:
        copy.wait()

    row = iota((rows, heads * hd), 0)
    block = iota((rows, heads * hd), 1) // hd
    q = jnp.where(block == row % heads, q, 0.0)
    half = heads * hd // 2
    q = q[:, :half] + q[:, half:]
    q = q + pltpu.roll(q, hd, 1)
    new_score = jnp.sum(q[:, :hd] * k_new, axis=1, keepdims=True) * hd**-0.5
    diagonal = block == (row // heads) % group
    q = jnp.where(diagonal, jnp.concatenate([q, q], axis=1) * hd**-0.5, 0.0).astype(bf16)
    head_row = iota(forget.shape, 0) % heads
    picked = iota(forget.shape, 1) == t * heads + head_row
    forget = jnp.sum(jnp.where(picked, forget, 0.0), axis=1, keepdims=True)
    log_forget = jnp.minimum(forget, 0.0) - jnp.log1p(jnp.exp(-jnp.abs(forget)))
    length = jnp.sum(
        jnp.where(repeat, lens[...].astype(f32), 0.0), axis=1, keepdims=True
    ).astype(jnp.int32)

    new_probs = []
    l_gates.wait()
    for g in range(n_groups):
        if g % chunk == 0:
            l_keys[g // chunk].wait()
        at = slice(g * gr, (g + 1) * gr)
        score = mm(q[at], keys[pl.ds(g * gk, gk), :])
        gate = jnp.concatenate([gates[g * group + n] for n in range(group)], axis=0)
        position = iota((gr, span), 1)
        latest = jnp.sum(
            jnp.where(position == length[at] - 1, gate, 0.0), axis=1, keepdims=True
        )
        score = score + (latest + log_forget[at]) - gate
        score = jnp.where(position < length[at], score, -jnp.inf)
        peak = jnp.maximum(jnp.max(score, axis=1, keepdims=True), new_score[at])
        past = jnp.exp(score - peak)
        new = jnp.exp(new_score[at] - peak)
        scale = 1.0 / (jnp.sum(past, axis=1, keepdims=True) + new)
        probs[pl.ds(g * gr, gr), :] = (past * scale).astype(bf16)
        new_probs.append((new * scale).astype(bf16).astype(f32))
    mixed = []
    for g in range(n_groups):
        if g % chunk == 0:
            l_vals[g // chunk].wait()
        mixed.append(mm_nt(probs[pl.ds(g * gr, gr), :], vals[pl.ds(g * gk, gk), :]))
    mixed = jnp.where(diagonal, jnp.concatenate(mixed, axis=0), 0.0)
    mixed = mixed[:, :half] + mixed[:, half:]
    mixed = mixed + pltpu.roll(mixed, hd, 1)
    mixed = mixed[:, :hd] + jnp.concatenate(new_probs, axis=0) * v_new
    spread = (iota((hd, heads * hd), 1) % hd) == iota((hd, heads * hd), 0)
    mixed = mm(mixed.astype(bf16), spread.astype(bf16))
    mixed = jnp.where(block == row % heads, mixed, 0.0).astype(bf16)
    gather = (iota((seqs, rows), 1) // heads) == iota((seqs, rows), 0)
    attended = mm(gather.astype(bf16), mixed).astype(bf16)

    l_wo.wait()
    pl.semaphore_wait(barrier, n_ep - 1 + n_tp - 1)
    copies = []
    order = [4, 5, 2, 6, 3, 7, 1]
    for n in order:
        to = tp_at(n // 2, n % 2)
        asend[n] = mm(attended, wo[:, pl.ds(pl.multiple_of(to * own, own), own)]).astype(bf16)
        copy = pltpu.make_async_remote_copy(
            asend.at[n], arecv.at[n], a_s.at[n], a_r.at[n],
            device_id={"tp": to}, device_id_type=MESH,
        )
        copy.start()
        copies.append(copy)
    own_cols = pl.ds(pl.multiple_of(t * own, own), own)
    stream = tok[:, own_cols].astype(f32)
    stream = stream + mm(attended, wo[:, own_cols]).astype(bf16).astype(f32)

    cols = 8 * n_ep
    lanes = own // 2
    q_at = iota((seqs, cols), 1)
    expert = (me + q_at // 8) % n_ep
    eye = iota((seqs, seqs), 0) == iota((seqs, seqs), 1)

    def column(ref, n):
        return jnp.sum(jnp.where(eye, ref[n : n + 1, :].astype(f32), 0.0), axis=1, keepdims=True)

    first = column(routes, 0).astype(jnp.int32) == expert
    second = column(routes, 1).astype(jnp.int32) == expert
    named = jnp.logical_or(first, second)
    before = iota((seqs, seqs), 1) < iota((seqs, seqs), 0)
    rank = mm(before.astype(bf16), named.astype(bf16))
    taken = jnp.logical_and(named, rank == (q_at % 4).astype(f32))
    l0, l1 = column(logits, 0), column(logits, 1)
    peak = jnp.maximum(l0, l1)
    e0 = jnp.exp(l0 - peak)
    e1 = jnp.exp(l1 - peak)
    weight = jnp.where(first, e0 / (e0 + e1), e1 / (e0 + e1))
    left = (q_at // 4) % 2 == 0
    slots = jnp.where(taken, 1.0, 0.0)
    slots = jnp.concatenate([jnp.where(left, slots, 0.0), jnp.where(left, 0.0, slots)], axis=0)
    combine = slots * jnp.concatenate([weight, weight], axis=0)
    dispatch = jnp.transpose(slots).astype(bf16)

    for copy in copies:
        copy.wait_recv()
    for n in order:
        stream = stream + arecv[n].astype(f32)

    sent = stream.astype(bf16)
    sent = jnp.concatenate([sent[:, :lanes], sent[:, lanes:]], axis=0)
    packed[...] = mm(dispatch, sent).astype(bf16).reshape(n_ep, 8, lanes)
    far = sorted(range(1, n_ep), key=lambda k: -(min(k // 4, 8 - k // 4) + min(k % 4, 4 - k % 4)))
    for k in far:
        pltpu.make_async_remote_copy(
            packed.at[k], arrived.at[k], d_s, d_r,
            device_id={"ep": (me + k) % n_ep}, device_id_type=MESH,
        ).start()
    arrived[0] = packed[0]
    rest = pl.ds(1, n_ep - 1)
    dispatched = pltpu.make_async_remote_copy(
        packed.at[rest], arrived.at[rest], d_s, d_r,
        device_id={"ep": (me + 1) % n_ep}, device_id_type=MESH,
    )
    dispatched.wait_recv()

    got = arrived[...].astype(f32).reshape(n_ep // 2, 2, 8, lanes)
    lo, hi = interleave(got[:, 0], got[:, 1])
    slot_rows = 4 * n_ep
    blocks[0] = jnp.concatenate(
        [lo.reshape(slot_rows, lanes), hi.reshape(slot_rows, lanes)], axis=1
    ).astype(bf16)
    g_copies = {}

    def gather_send(src, dst, to):
        copy = pltpu.make_async_remote_copy(
            blocks.at[src], blocks.at[dst], g_s.at[dst], g_r.at[dst],
            device_id={"tp": to}, device_id_type=MESH,
        )
        copy.start()
        g_copies[dst] = copy

    for dy in (2, 1, 3):
        gather_send(0, 2 * dy, tp_at(dy, 0))
    gather_send(0, 1, tp_at(0, 1))
    l_wg.wait()
    l_wu.wait()
    gate_act = upper = squares = None
    for n in (0, 1, 2, 6, 3, 7, 4, 5):
        if n:
            g_copies[n].wait_recv()
        if n in (2, 6, 4):
            gather_send(n, n + 1, tp_at(0, 1))
        cols_n = pl.ds(pl.multiple_of(tp_from(n // 2, n % 2) * own, own), own)
        part = blocks[n].astype(f32)
        square = jnp.sum(part * part, axis=1, keepdims=True)
        part = (part * pgain[:, cols_n]).astype(bf16)
        gate_part = mm_nt(part, wg[:, cols_n])
        upper_part = mm_nt(part, wu[:, cols_n])
        gate_act = gate_part if n == 0 else gate_act + gate_part
        upper = upper_part if n == 0 else upper + upper_part
        squares = square if n == 0 else squares + square
    norm = lax.rsqrt(squares / width + EPSILON)
    gate_act = gate_act * norm
    hidden = ((gate_act / (1.0 + jnp.exp(-gate_act))) * (upper * norm)).astype(bf16)

    l_wd.wait()

    def down(dy, dc):
        at = pl.ds(pl.multiple_of(tp_at(dy, dc) * own, own), own)
        return mm(hidden, wd[:, at])

    p_copies = {}
    for dy in (2, 1, 3, 0):
        psend[dy] = down(dy, 1).astype(bf16)
        copy = pltpu.make_async_remote_copy(
            psend.at[dy], precv.at[dy], p_s.at[dy], p_r.at[dy],
            device_id={"tp": tp_at(0, 1)}, device_id_type=MESH,
        )
        copy.start()
        p_copies[dy] = copy
    t_copies = {}
    for dy in (2, 1, 3, 0):
        part = down(dy, 0)
        p_copies[dy].wait_recv()
        part = part + precv[dy].astype(f32)
        if dy == 0:
            total = part
        else:
            tsend[dy] = part.astype(bf16)
            copy = pltpu.make_async_remote_copy(
                tsend.at[dy], trecv.at[dy], t_s.at[dy], t_r.at[dy],
                device_id={"tp": tp_at(dy, 0)}, device_id_type=MESH,
            )
            copy.start()
            t_copies[dy] = copy
    for dy in (1, 3, 2):
        t_copies[dy].wait_recv()
        total = total + trecv[dy].astype(f32)

    lo, hi = interleave(
        total[:, :lanes].reshape(n_ep // 2, 8, lanes), total[:, lanes:].reshape(n_ep // 2, 8, lanes)
    )
    ret_send[...] = jnp.stack([lo, hi], axis=1).reshape(n_ep, 8, lanes).astype(bf16)
    for k in far:
        pltpu.make_async_remote_copy(
            ret_send.at[k], ret.at[k], b_s, b_r,
            device_id={"ep": (me + n_ep - k) % n_ep}, device_id_type=MESH,
        ).start()
    ret[0] = ret_send[0]
    high = combine.astype(bf16)
    left_over = combine - high.astype(f32)
    mid = left_over.astype(bf16)
    low = (left_over - mid.astype(f32)).astype(bf16)
    returned = pltpu.make_async_remote_copy(
        ret_send.at[rest], ret.at[rest], b_s, b_r,
        device_id={"ep": (me + n_ep - 1) % n_ep}, device_id_type=MESH,
    )
    returned.wait_recv()
    back = ret[...].reshape(cols, lanes)
    mix = mm(high, back) + mm(mid, back) + mm(low, back)
    out_ref[:, :lanes] = (stream[:, :lanes] + mix[:seqs]).astype(bf16)
    out_ref[:, lanes:] = (stream[:, lanes:] + mix[seqs:]).astype(bf16)

    for copy in copies:
        copy.wait_send()
    dispatched.wait_send()
    for some in (g_copies, p_copies, t_copies):
        for copy in some.values():
            copy.wait_send()
    returned.wait_send()


def body(n_ep, n_tp, *args):
    (
        tokens, norm_gain, post_gain, w_query, w_key, w_value, w_forget, w_output,
        key_cache, value_cache, gate_cache, lengths, routes, route_logits, w_gate, w_up, w_down,
    ) = args
    seqs, width = tokens.shape
    hd, span = key_cache.shape[2:]
    heads = gate_cache.shape[1]
    own = width // n_tp
    operands = (
        tokens, norm_gain.reshape(1, width), post_gain.reshape(1, width),
        w_query, w_key.T, w_value.T, w_forget.T, w_output,
        key_cache.reshape(seqs * hd, span), value_cache.reshape(seqs * hd, span), gate_cache,
        lengths.reshape(1, seqs), routes.T, route_logits.T, w_gate[0].T, w_up[0].T, w_down[0],
    )
    slots = 4 * n_ep
    dma = pltpu.SemaphoreType.DMA
    scratch = [pltpu.VMEM(a.shape, a.dtype) for a in operands] + [
        pltpu.VMEM((seqs * heads, span), bf16),
        pltpu.VMEM((n_tp, seqs, own), bf16),
        pltpu.VMEM((n_tp, seqs, own), bf16),
        pltpu.VMEM((n_ep, 8, own // 2), bf16),
        pltpu.VMEM((n_ep, 8, own // 2), bf16),
        pltpu.VMEM((n_tp, slots, own), bf16),
        pltpu.VMEM((n_tp // 2, slots, own), bf16),
        pltpu.VMEM((n_tp // 2, slots, own), bf16),
        pltpu.VMEM((n_tp // 2, slots, own), bf16),
        pltpu.VMEM((n_tp // 2, slots, own), bf16),
        pltpu.VMEM((n_ep, 8, own // 2), bf16),
        pltpu.VMEM((n_ep, 8, own // 2), bf16),
        dma((32,)),
        dma((n_tp,)), dma((n_tp,)),
        dma, dma,
        dma((n_tp,)), dma((n_tp,)),
        dma((n_tp // 2,)), dma((n_tp // 2,)),
        dma((n_tp // 2,)), dma((n_tp // 2,)),
        dma, dma,
    ]
    return pl.pallas_call(
        functools.partial(kernel, n_ep, n_tp),
        out_shape=jax.ShapeDtypeStruct((seqs, own), bf16),
        in_specs=[pl.BlockSpec(memory_space=pl.ANY)] * len(operands),
        out_specs=pl.BlockSpec(memory_space=pltpu.VMEM),
        scratch_shapes=scratch,
        compiler_params=pltpu.CompilerParams(
            collective_id=0, has_side_effects=True, vmem_limit_bytes=60 * 1024 * 1024
        ),
        name="layer",
    )(*operands)


def solution(mesh):
    in_specs = (
        P("ep", None),
        P(),
        P(),
        P(None, "tp"),
        P(None, "tp"),
        P(None, "tp"),
        P(),
        P("tp", None),
        P("ep", "tp", None, None),
        P("ep", "tp", None, None),
        P("ep", "tp", None),
        P("ep"),
        P("ep", None),
        P("ep", None),
        P("ep", None, "tp"),
        P("ep", None, "tp"),
        P("ep", "tp", None),
    )
    step = functools.partial(body, mesh.shape["ep"], mesh.shape["tp"])
    return jax.shard_map(
        step, mesh=mesh, in_specs=in_specs, out_specs=P("ep", "tp"), check_vma=False
    )
```

time: 102 us -> 44.7 us (0.44)
  Pallas kernels: 0 us -> 43.2 us
  waiting for transfers between devices: 32.1 us -> 0 us
  blocking collectives: 25.5 us -> 0 us
  starting transfers between devices: 17.9 us -> 0 us
  matrix products: 15.7 us -> 0 us
  other arithmetic: 5.17 us -> 0 us
  local copies, waits for them, and re-layouts: 4.44 us -> 1.32 us
    pallas_call x0 -> x1, Pallas kernels: none -> 43.2 us  [body(): pl.pallas_call(functools.partial(kernel, n_ep, n_tp), out_shape=jax.Shape...]
    all_to_all x3 -> x0, waiting for transfers between devices: 32.1 us -> none  [the longest x1 14.4 us: copy_for_each(): return lax.all_to_all(copies, axis, split_axis=0, concat_axis=0, tiled=True)]
    all_to_all x1 -> x0, blocking collectives: 25.5 us -> none  [body(): lax.all_to_all(packed.reshape(ep_count, capacity, sent_width), 'ep', spli...]
    all_to_all x3 -> x0, starting transfers between devices: 17.9 us -> none  [the longest x1 6.79 us: copy_for_each(): return lax.all_to_all(copies, axis, split_axis=0, concat_axis=0, tiled=True)]
    dot_general x13 -> x0, matrix products: 15.7 us -> none  [the longest x1 3.14 us: body(): jnp.einsum('bkgd,bkdl->bkgl', query_vector, key_cache, preferred_element_...]
    reduce_sum x8 -> x0, other arithmetic: 3.24 us -> none  [the longest x1 1.31 us: body(): jnp.sum(jnp.where(cache_position == last_index, gate_cache, 0.0), axis=-1)]
    reshape x7 -> x0, local copies, waits for them, and re-layouts: 2.02 us -> none  [the longest x1 0.82 us: cut_along(): array.reshape(*shape[:dim], count, shape[dim] // count, *shape[dim + 1:])]
    broadcast_in_dim x1 -> x0, local copies, waits for them, and re-layouts: 1.11 us -> none  [copy_for_each(): copies = jnp.broadcast_to(array, (lax.axis_size(axis), *array.shape))]
  transfers between devices with their start and end apart: 3 -> 0, of which waited for: 3 -> 0; matrix products, arithmetic and copies ran while one was open for 1% -> 0% of each run, Pallas kernels for 0% -> 0%
where the time goes in v1:
time: 44.7 us; the launch traced here: 44.6 us
  Pallas kernels  43.2 us (97%)
  local copies, waits for them, and re-layouts  1.32 us (3%)
    pallas_call x1, Pallas kernels, body(): pl.pallas_call(functools.partial(kernel, n_ep, n_tp), out_shape=jax.Shape...  43.2 us
    unnamed x1, local copies, waits for them, and re-layouts  1.32 us

profile of v1, /device:TPU:1, one launch (start us, length us, event | category | flops | bytes accessed | tf_op | source)
XLA Modules:
  0.0 44.6 jit_solution(2849260734626958665)
XLA Ops:
  0.0 43.2 %layer.1 = bf16[32,256]{1,0:T(8,128)(2,1)} custom-call(bf16[32,2048]{1,0:T(8,128)(2,1)} %refs_0_.1, f32[1,2048]{1,0:T(1,128)} %bitcast.25, f32[1,2048]{1,0:T(1,128)} %bitcast.26, bf16[2048,256]{1,0:T(8,128)(2,1)} %refs_3_.1, bf16[64,2048]{1,0:T(8,128)(2,1)} %bitcast.22, bf16[64,2048]{1,0:T(8,128)(2,1)} %bitcast.23, bf16[32,2048]{1,0:T(8,128)(2,1)} %bitcast.24, ...), custom_call_target="tpu_custom_call" | custom-call | tf_op jit(solution)/shard_map/layer/pallas_call | solution.py:383
  43.2 1.3 %copy.19 = bf16[32,256]{1,0:T(8,128)(2,1)} copy(bf16[32,256]{1,0:T(8,128)(2,1)} %layer.1) | data formatting | bytes 32768

commit v2 on v1

v2 whole, which is shorter than its diff:
```python
import functools

import jax
import jax.numpy as jnp
from jax import lax
from jax.experimental import pallas as pl
from jax.experimental.pallas import tpu as pltpu
from jax.sharding import PartitionSpec as P

f32 = jnp.float32
bf16 = jnp.bfloat16
MESH = pl.DeviceIdType.MESH
EPSILON = 1e-06
NX = 4


def mm(a, b):
    return jnp.dot(a, b, preferred_element_type=f32)


def mm_nt(a, b):
    return lax.dot_general(a, b, (((1,), (1,)), ((), ())), preferred_element_type=f32)


def iota(shape, dim):
    return lax.broadcasted_iota(jnp.int32, shape, dim)


def interleave(even, odd):
    low = iota(even.shape, 1) < 4
    first = jnp.where(low, even, pltpu.roll(odd, 4, 1))
    second = jnp.where(low, pltpu.roll(even, 4, 1), odd)
    return first, second


def kernel(n_ep, n_tp, *refs):
    hbm = refs[:17]
    out_ref = refs[17]
    (
        tok, ngain, pgain, wq, wkvf, wo, keys, vals, gates, lens, routes, logits, wg, wu, wd,
    ) = refs[18:33]
    (
        probs, asend, arecv, packed, arrived, blocks, psend, precv, tsend, trecv, ret_send, ret,
        load_sem, a_s, a_r, d_s, d_r, g_s, g_r, p_s, p_r, t_s, t_r, b_s, b_r,
    ) = refs[33:]
    n_y = n_tp // 2
    me = lax.axis_index("ep")
    t = lax.axis_index("tp")
    y = t // 2
    c = t % 2
    seqs, width = tok.shape
    heads = gates.shape[1]
    rows = seqs * heads
    span = keys.shape[1]
    hd = keys.shape[0] // seqs
    own = width // n_tp

    n_z = n_ep // NX
    z = me // NX
    xx = me % NX
    near = 5 * NX
    offsets = [(kz, kx) for kz in (0, 1, 2, 6, 7, 3, 4, 5) for kx in range(NX)]

    def ep_at(p, sign=1):
        kz, kx = offsets[p]
        if sign < 0:
            kz, kx = n_z - kz, NX - kx
        return ((z + kz) % n_z) * NX + (xx + kx) % NX

    def tp_at(dy, dc):
        return ((y + dy) % n_y) * 2 + (c if dc == 0 else 1 - c)

    def tp_from(dy, dc):
        return ((y + n_y - dy) % n_y) * 2 + (c if dc == 0 else 1 - c)

    def load(n, dst, part=None, into=None):
        src = hbm[n]
        if part is not None:
            src, dst = src.at[part], dst.at[part]
        if into is not None:
            dst = dst.at[pl.ds(into, src.shape[0])]
        load.count += 1
        copy = pltpu.make_async_copy(src, dst, load_sem.at[load.count - 1])
        copy.start()
        return copy

    load.count = 0
    group = 4
    n_groups = seqs // group
    gr = group * heads
    gk = group * hd
    chunk = 2
    slices = [pl.ds(n * chunk * gk, chunk * gk) for n in range(n_groups // chunk)]
    l_tok = load(0, tok)
    l_ngain = load(1, ngain)
    l_wq = load(3, wq)
    l_kvf = [load(4, wkvf, into=0), load(5, wkvf, into=hd), load(6, wkvf, into=2 * hd)]
    l_small = [load(11, lens), load(12, routes), load(13, logits), load(2, pgain)]
    l_gates = load(10, gates)
    l_keys, l_vals = [], []
    for s in slices:
        l_keys.append(load(8, keys, s))
        l_vals.append(load(9, vals, s))
    l_wo = load(7, wo)
    l_wg = load(14, wg)
    l_wu = load(15, wu)
    l_wd = load(16, wd)

    barrier = pltpu.get_barrier_semaphore()
    for k in range(1, n_ep):
        pl.semaphore_signal(
            barrier, inc=1, device_id={"ep": ep_at(k)}, device_id_type=MESH
        )
    for n in range(1, n_tp):
        pl.semaphore_signal(
            barrier, inc=1, device_id={"tp": tp_at(n // 2, n % 2)}, device_id_type=MESH
        )

    l_tok.wait()
    l_ngain.wait()
    x = tok[...].astype(f32)
    normed = x * lax.rsqrt(jnp.mean(x * x, axis=-1, keepdims=True) + EPSILON) * ngain[...]
    repeat = (iota((rows, seqs), 0) // heads) == iota((rows, seqs), 1)
    normed = mm(repeat.astype(bf16), normed.astype(bf16)).astype(bf16)
    l_wq.wait()
    q = mm(normed, wq[...]).astype(bf16).astype(f32)
    for copy in l_kvf:
        copy.wait()
    kvf = mm_nt(normed, wkvf[...])
    k_new = kvf[:, :hd].astype(bf16).astype(f32)
    v_new = kvf[:, hd : 2 * hd].astype(bf16).astype(f32)
    forget = kvf[:, 2 * hd :]
    for copy in l_small:
        copy.wait()

    row = iota((rows, heads * hd), 0)
    block = iota((rows, heads * hd), 1) // hd
    q = jnp.where(block == row % heads, q, 0.0)
    half = heads * hd // 2
    q = q[:, :half] + q[:, half:]
    q = q + pltpu.roll(q, hd, 1)
    new_score = jnp.sum(q[:, :hd] * k_new, axis=1, keepdims=True) * hd**-0.5
    diagonal = block == (row // heads) % group
    q = jnp.where(diagonal, jnp.concatenate([q, q], axis=1) * hd**-0.5, 0.0).astype(bf16)
    head_row = iota(forget.shape, 0) % heads
    picked = iota(forget.shape, 1) == t * heads + head_row
    forget = jnp.sum(jnp.where(picked, forget, 0.0), axis=1, keepdims=True)
    log_forget = jnp.minimum(forget, 0.0) - jnp.log1p(jnp.exp(-jnp.abs(forget)))
    length = jnp.sum(
        jnp.where(repeat, lens[...].astype(f32), 0.0), axis=1, keepdims=True
    ).astype(jnp.int32)

    new_probs, mixed = [], []
    l_gates.wait()

    def weigh(g):
        mixed.append(mm_nt(probs[pl.ds(g * gr, gr), :], vals[pl.ds(g * gk, gk), :]))

    for g in range(n_groups):
        if g % chunk == 0:
            l_keys[g // chunk].wait()
        at = slice(g * gr, (g + 1) * gr)
        score = mm(q[at], keys[pl.ds(g * gk, gk), :])
        if g >= chunk:
            if g % chunk == 0:
                l_vals[g // chunk - 1].wait()
            weigh(g - chunk)
        gate = jnp.concatenate([gates[g * group + n] for n in range(group)], axis=0)
        position = iota((gr, span), 1)
        latest = jnp.sum(
            jnp.where(position == length[at] - 1, gate, 0.0), axis=1, keepdims=True
        )
        score = score + (latest + log_forget[at]) - gate
        score = jnp.where(position < length[at], score, -jnp.inf)
        peak = jnp.maximum(jnp.max(score, axis=1, keepdims=True), new_score[at])
        past = jnp.exp(score - peak)
        new = jnp.exp(new_score[at] - peak)
        scale = 1.0 / (jnp.sum(past, axis=1, keepdims=True) + new)
        probs[pl.ds(g * gr, gr), :] = (past * scale).astype(bf16)
        new_probs.append((new * scale).astype(bf16).astype(f32))
    l_vals[-1].wait()
    for g in range(n_groups - chunk, n_groups):
        weigh(g)
    mixed = jnp.where(diagonal, jnp.concatenate(mixed, axis=0), 0.0)
    mixed = mixed[:, :half] + mixed[:, half:]
    mixed = mixed + pltpu.roll(mixed, hd, 1)
    mixed = mixed[:, :hd] + jnp.concatenate(new_probs, axis=0) * v_new
    spread = (iota((hd, heads * hd), 1) % hd) == iota((hd, heads * hd), 0)
    mixed = mm(mixed.astype(bf16), spread.astype(bf16))
    mixed = jnp.where(block == row % heads, mixed, 0.0).astype(bf16)
    gather = (iota((seqs, rows), 1) // heads) == iota((seqs, rows), 0)
    attended = mm(gather.astype(bf16), mixed).astype(bf16)

    l_wo.wait()
    partial = mm(attended, wo[...]).astype(bf16)
    for n in range(n_tp):
        asend[n] = partial[:, n * own : (n + 1) * own]
    pl.semaphore_wait(barrier, n_ep - 1 + n_tp - 1)
    copies = []
    order = [4, 5, 2, 6, 3, 7, 1]
    for n in order:
        to = tp_at(n // 2, n % 2)
        copy = pltpu.make_async_remote_copy(
            asend.at[to], arecv.at[n], a_s.at[n], a_r.at[n],
            device_id={"tp": to}, device_id_type=MESH,
        )
        copy.start()
        copies.append(copy)
    own_cols = pl.ds(pl.multiple_of(t * own, own), own)
    stream = tok[:, own_cols].astype(f32) + asend[t].astype(f32)

    cols = 8 * n_ep
    lanes = own // 2
    q_at = iota((seqs, cols), 1)
    pz = q_at >> 5
    pz = jnp.where(pz < 3, pz, jnp.where(pz < 5, pz + 3, pz - 2))
    expert = ((z + pz) & (n_z - 1)) * NX + ((xx + (q_at >> 3)) & (NX - 1))
    eye = iota((seqs, seqs), 0) == iota((seqs, seqs), 1)

    def column(ref, n):
        return jnp.sum(jnp.where(eye, ref[n : n + 1, :].astype(f32), 0.0), axis=1, keepdims=True)

    first = column(routes, 0).astype(jnp.int32) == expert
    second = column(routes, 1).astype(jnp.int32) == expert
    named = jnp.logical_or(first, second)
    before = iota((seqs, seqs), 1) < iota((seqs, seqs), 0)
    rank = mm(before.astype(bf16), named.astype(bf16))
    taken = jnp.logical_and(named, rank == (q_at & 3).astype(f32))
    l0, l1 = column(logits, 0), column(logits, 1)
    peak = jnp.maximum(l0, l1)
    e0 = jnp.exp(l0 - peak)
    e1 = jnp.exp(l1 - peak)
    weight = jnp.where(first, e0 / (e0 + e1), e1 / (e0 + e1))
    left = (q_at & 4) == 0
    slots = jnp.where(taken, 1.0, 0.0)
    slots = jnp.concatenate([jnp.where(left, slots, 0.0), jnp.where(left, 0.0, slots)], axis=0)
    combine = slots * jnp.concatenate([weight, weight], axis=0)
    dispatch = jnp.transpose(slots).astype(bf16)

    for copy in copies:
        copy.wait_recv()
    for n in order:
        stream = stream + arecv[n].astype(f32)

    sent = stream.astype(bf16)
    sent = jnp.concatenate([sent[:, :lanes], sent[:, lanes:]], axis=0)
    packed[...] = mm(dispatch, sent).astype(bf16).reshape(n_ep, 8, lanes)
    spans = [range(1, near), range(near, n_ep)]

    def over_ep(src, dst, send, recv, part, sign):
        for p in reversed(spans[part]):
            pltpu.make_async_remote_copy(
                src.at[p], dst.at[p], send.at[part], recv.at[part],
                device_id={"ep": ep_at(p, sign)}, device_id_type=MESH,
            ).start()
        at = pl.ds(spans[part][0], len(spans[part]))
        return pltpu.make_async_remote_copy(
            src.at[at], dst.at[at], send.at[part], recv.at[part],
            device_id={"ep": ep_at(1, sign)}, device_id_type=MESH,
        )

    FAR, NEAR = 1, 0
    dispatched = {part: over_ep(packed, arrived, d_s, d_r, part, 1) for part in (FAR, NEAR)}
    arrived[0] = packed[0]

    first_block = [0, near]
    block_count = [near, n_ep - near]
    row_span = [pl.ds(4 * first_block[part], 4 * block_count[part]) for part in (NEAR, FAR)]
    g_copies = {}

    def gather_send(part, src, dst, to):
        copy = pltpu.make_async_remote_copy(
            blocks.at[src, row_span[part]], blocks.at[dst, row_span[part]],
            g_s.at[part, dst], g_r.at[part, dst],
            device_id={"tp": to}, device_id_type=MESH,
        )
        copy.start()
        g_copies[part, dst] = copy

    def take(part):
        dispatched[part].wait_recv()
        count = block_count[part]
        got = arrived[pl.ds(first_block[part], count)].astype(f32)
        got = got.reshape(count // 2, 2, 8, lanes)
        lo, hi = interleave(got[:, 0], got[:, 1])
        blocks[0, row_span[part], :] = jnp.concatenate(
            [lo.reshape(4 * count, lanes), hi.reshape(4 * count, lanes)], axis=1
        ).astype(bf16)
        for dy in (2, 1, 3):
            gather_send(part, 0, 2 * dy, tp_at(dy, 0))
        gather_send(part, 0, 1, tp_at(0, 1))

    take(NEAR)
    take(FAR)
    l_wg.wait()
    l_wu.wait()
    sums = [None, None, None]

    def expand(n):
        cols_n = pl.ds(pl.multiple_of(tp_from(n // 2, n % 2) * own, own), own)
        part = blocks[n].astype(f32)
        square = jnp.sum(part * part, axis=1, keepdims=True)
        part = (part * pgain[:, cols_n]).astype(bf16)
        for at, add in enumerate((mm_nt(part, wg[:, cols_n]), mm_nt(part, wu[:, cols_n]), square)):
            sums[at] = add if sums[at] is None else sums[at] + add

    def hear(part, n):
        g_copies[part, n].wait_recv()
        if n in (2, 4, 6):
            gather_send(part, n, n + 1, tp_at(0, 1))

    for n in (1, 2, 6):
        hear(NEAR, n)
    expand(0)
    hear(FAR, 1)
    expand(1)
    hear(NEAR, 4)
    hear(FAR, 2)
    hear(NEAR, 3)
    expand(2)
    hear(FAR, 6)
    hear(NEAR, 7)
    expand(6)
    hear(FAR, 4)
    hear(NEAR, 5)
    for n in (3, 7, 4, 5):
        if n != 4:
            hear(FAR, n)
        expand(n)
    gate_act, upper, squares = sums
    norm = lax.rsqrt(squares / width + EPSILON)
    gate_act = gate_act * norm
    hidden = ((gate_act / (1.0 + jnp.exp(-gate_act))) * (upper * norm)).astype(bf16)

    l_wd.wait()

    def down(dy, dc):
        at = pl.ds(pl.multiple_of(tp_at(dy, dc) * own, own), own)
        return mm(hidden, wd[:, at])

    p_copies = {}
    for some in ((2,), (1, 3, 0)):
        for dy in some:
            psend[dy] = down(dy, 1).astype(bf16)
        for dy in some:
            p_copies[dy] = pltpu.make_async_remote_copy(
                psend.at[dy], precv.at[dy], p_s.at[dy], p_r.at[dy],
                device_id={"tp": tp_at(0, 1)}, device_id_type=MESH,
            )
            p_copies[dy].start()
    parts = {dy: down(dy, 0) for dy in (2, 1, 3, 0)}
    t_copies = {}

    def along_y(part, dy):
        at = row_span[part]
        t_copies[part, dy] = pltpu.make_async_remote_copy(
            tsend.at[dy, at], trecv.at[dy, at], t_s.at[part, dy], t_r.at[part, dy],
            device_id={"tp": tp_at(dy, 0)}, device_id_type=MESH,
        )
        t_copies[part, dy].start()

    for dy in (2, 1, 3):
        p_copies[dy].wait_recv()
        tsend[dy] = (parts[dy] + precv[dy].astype(f32)).astype(bf16)
        along_y(FAR, dy)
    for dy in (2, 1, 3):
        along_y(NEAR, dy)
    p_copies[0].wait_recv()
    total = parts[0] + precv[0].astype(f32)

    returned = {}

    def give_back(part):
        for dy in (1, 3, 2):
            t_copies[part, dy].wait_recv()
        count = block_count[part]
        rows_at = slice(4 * first_block[part], 4 * (first_block[part] + count))
        mine = total[rows_at]
        for dy in (1, 3, 2):
            mine = mine + trecv[dy, row_span[part], :].astype(f32)
        lo, hi = interleave(
            mine[:, :lanes].reshape(count // 2, 8, lanes), mine[:, lanes:].reshape(count // 2, 8, lanes)
        )
        ret_send[pl.ds(first_block[part], count)] = (
            jnp.stack([lo, hi], axis=1).reshape(count, 8, lanes).astype(bf16)
        )
        returned[part] = over_ep(ret_send, ret, b_s, b_r, part, -1)

    give_back(FAR)
    give_back(NEAR)
    ret[0] = ret_send[0]
    high = combine.astype(bf16)
    left_over = combine - high.astype(f32)
    mid = left_over.astype(bf16)
    low = (left_over - mid.astype(f32)).astype(bf16)
    for part in (NEAR, FAR):
        returned[part].wait_recv()
    back = ret[...].reshape(cols, lanes)
    mix = mm(high, back) + mm(mid, back) + mm(low, back)
    out_ref[:, :lanes] = (stream[:, :lanes] + mix[:seqs]).astype(bf16)
    out_ref[:, lanes:] = (stream[:, lanes:] + mix[seqs:]).astype(bf16)

    for copy in copies:
        copy.wait_send()
    for some in (dispatched, g_copies, p_copies, t_copies, returned):
        for copy in some.values():
            copy.wait_send()


def body(n_ep, n_tp, *args):
    (
        tokens, norm_gain, post_gain, w_query, w_key, w_value, w_forget, w_output,
        key_cache, value_cache, gate_cache, lengths, routes, route_logits, w_gate, w_up, w_down,
    ) = args
    seqs, width = tokens.shape
    hd, span = key_cache.shape[2:]
    heads = gate_cache.shape[1]
    own = width // n_tp
    operands = (
        tokens, norm_gain.reshape(1, width), post_gain.reshape(1, width),
        w_query, w_key.T, w_value.T, w_forget.T, w_output,
        key_cache.reshape(seqs * hd, span), value_cache.reshape(seqs * hd, span), gate_cache,
        lengths.reshape(1, seqs), routes.T, route_logits.T, w_gate[0].T, w_up[0].T, w_down[0],
    )
    slots = 4 * n_ep
    dma = pltpu.SemaphoreType.DMA
    kvf_rows = operands[4].shape[0] + operands[5].shape[0] + operands[6].shape[0]
    kvf = jax.ShapeDtypeStruct((kvf_rows, width), bf16)
    held = operands[:4] + (kvf,) + operands[7:]
    scratch = [pltpu.VMEM(a.shape, a.dtype) for a in held] + [
        pltpu.VMEM((seqs * heads, span), bf16),
        pltpu.VMEM((n_tp, seqs, own), bf16),
        pltpu.VMEM((n_tp, seqs, own), bf16),
        pltpu.VMEM((n_ep, 8, own // 2), bf16),
        pltpu.VMEM((n_ep, 8, own // 2), bf16),
        pltpu.VMEM((n_tp, slots, own), bf16),
        pltpu.VMEM((n_tp // 2, slots, own), bf16),
        pltpu.VMEM((n_tp // 2, slots, own), bf16),
        pltpu.VMEM((n_tp // 2, slots, own), bf16),
        pltpu.VMEM((n_tp // 2, slots, own), bf16),
        pltpu.VMEM((n_ep, 8, own // 2), bf16),
        pltpu.VMEM((n_ep, 8, own // 2), bf16),
        dma((32,)),
        dma((n_tp,)), dma((n_tp,)),
        dma((2,)), dma((2,)),
        dma((2, n_tp)), dma((2, n_tp)),
        dma((n_tp // 2,)), dma((n_tp // 2,)),
        dma((2, n_tp // 2)), dma((2, n_tp // 2)),
        dma((2,)), dma((2,)),
    ]
    return pl.pallas_call(
        functools.partial(kernel, n_ep, n_tp),
        out_shape=pltpu.VMEM((seqs, own), bf16),
        in_specs=[pl.BlockSpec(memory_space=pltpu.HBM)] * len(operands),
        out_specs=pl.BlockSpec(memory_space=pltpu.VMEM),
        scratch_shapes=scratch,
        compiler_params=pltpu.CompilerParams(
            collective_id=0, has_side_effects=True, vmem_limit_bytes=54 * 1024 * 1024
        ),
        name="layer",
    )(*operands)


def solution(mesh):
    in_specs = (
        P("ep", None),
        P(),
        P(),
        P(None, "tp"),
        P(None, "tp"),
        P(None, "tp"),
        P(),
        P("tp", None),
        P("ep", "tp", None, None),
        P("ep", "tp", None, None),
        P("ep", "tp", None),
        P("ep"),
        P("ep", None),
        P("ep", None),
        P("ep", None, "tp"),
        P("ep", None, "tp"),
        P("ep", "tp", None),
    )
    step = functools.partial(body, mesh.shape["ep"], mesh.shape["tp"])
    return jax.shard_map(
        step, mesh=mesh, in_specs=in_specs, out_specs=P("ep", "tp"), check_vma=False
    )
```

time: 44.7 us -> 41.3 us (0.924)
  Pallas kernels: 43.2 us -> 40.6 us
  local copies, waits for them, and re-layouts: 1.32 us -> 0.61 us
    pallas_call x1, Pallas kernels: 43.2 us -> 40.6 us  [body(): pl.pallas_call(functools.partial(kernel, n_ep, n_tp), out_shape=pltpu.VME...]
    unnamed x1, local copies, waits for them, and re-layouts: 1.32 us -> 0.61 us
where the time goes in v2:
time: 41.3 us; the launch traced here: 41.2 us
  Pallas kernels  40.6 us (98%)
  local copies, waits for them, and re-layouts  0.61 us (1%)
    pallas_call x1, Pallas kernels, body(): pl.pallas_call(functools.partial(kernel, n_ep, n_tp), out_shape=pltpu.VME...  40.6 us

profile of v2, /device:TPU:1, one launch (start us, length us, event | category | flops | bytes accessed | tf_op | source)
XLA Modules:
  0.0 41.2 jit_solution(4364389682249519613)
XLA Ops:
  0.0 40.6 %layer.1 = bf16[32,256]{1,0:T(8,128)(2,1)S(1)} custom-call(bf16[32,2048]{1,0:T(8,128)(2,1)} %refs_0_.1, f32[1,2048]{1,0:T(1,128)} %bitcast.25, f32[1,2048]{1,0:T(1,128)} %bitcast.26, bf16[2048,256]{1,0:T(8,128)(2,1)} %refs_3_.1, bf16[64,2048]{1,0:T(8,128)(2,1)} %bitcast.22, bf16[64,2048]{1,0:T(8,128)(2,1)} %bitcast.23, bf16[32,2048]{1,0:T(8,128)(2,1)} %bitcast.24, ...), custom_call_target="tpu_custom_call" | custom-call | tf_op jit(solution)/shard_map/layer/pallas_call | solution.py:451
  40.6 0.6 %copy.19 = bf16[32,256]{1,0:T(8,128)(2,1)} copy(bf16[32,256]{1,0:T(8,128)(2,1)S(1)} %layer.1) | data formatting | bytes 32768
